TPU v7x, 32 devices: a whole 2x2x4 slice. The times are simulated.
32 devices in a mesh: sp: 8 (over z, core), tp: 4 (over y, x).
Axes of the slice: x: 2, y: 2, z: 4, core: 2. Of those that a mesh axis runs over, the one named last changes fastest.
Arguments:
- tokens: bfloat16 [6144, 2048], P('sp', 'tp'), may hold values from -26 to 26, as said below
- mix_gain: bfloat16 [2, 2048], replicated, may hold values from 0.099609375 to 1.8984375
- x_weight: bfloat16 [2, 2048, 1024], P(None, 'sp', 'tp'), may hold values from -0.125 to 0.125
- gate_weight: bfloat16 [2, 2048, 1024], P(None, 'sp', 'tp'), may hold values from -0.125 to 0.125
- conv_taps: bfloat16 [2, 4, 1024], P(None, None, 'tp'), may hold values from -3 to 3
- a_maps: bfloat16 [2, 16, 64, 64], P(None, 'tp'), may hold values from -0.75 to 0.75
- i_maps: bfloat16 [2, 16, 64, 64], P(None, 'tp'), may hold values from -0.75 to 0.75
- decay_rate: float32 [2, 1024], P(None, 'tp'), as said below
- pace: float32 [6144], P('sp'), may hold values from 0.35 to 2.8, as said below
- jumps: float32 [6144], P('sp'), may hold values from -0.7 to 0, as said below
- out_gain: bfloat16 [2, 1024], P(None, 'tp'), may hold values from 0.099609375 to 1.8984375
- out_weight: bfloat16 [2, 1024, 2048], P(None, 'sp', 'tp'), may hold values from -0.1875 to 0.1875
Outputs:
- stream: bfloat16 [6144, 2048], P('sp', 'tp')
Inputs may be any that keep to these rules, and one draw needn't show every extreme that they name: `tokens`: random-looking real values; feature scales differ along the features. `decay_rate`: positive. `pace`: positive. `jumps`: zero or negative.
All inputs are finite; a program needn't handle non-finite values.
Results may differ from a plain program's by a relative error of at most 0.01.
Values may be sent and summed in bfloat16 or wider, within the bound.
A program may use at most 64 MiB of HBM per device.

v0:
```python
import jax
import jax.numpy as jnp
from jax import lax
from jax.sharding import PartitionSpec as P

D_REC = 1024
HEAD = 64
WIDTH = 4
LAYERS = 2


EPS = 1e-06
GATE_C = 8.0


def from_behind(x, axis, by):
    peers = lax.axis_size(axis)
    pairs = [(i, i + by) for i in range(peers) if 0 <= i + by < peers]
    return lax.ppermute(x, axis, pairs)


def prefix(part, axis, combine, identity):
    place = lax.axis_index(axis)
    gathered = jax.tree.map(lambda a: lax.all_gather(a, axis), part)
    state = jax.tree.map(lambda a, e: jnp.zeros_like(a) + jnp.asarray(e, a.dtype), part, identity)

    def one(hop, state):
        return combine(
            state, jax.tree.map(lambda a: lax.dynamic_index_in_dim(a, hop, 0, False), gathered)
        )

    return lax.fori_loop(0, place, one, state)


def combine(first, second):
    return (first[0] * second[0], second[0] * first[1] + second[1])


def body(
    tokens,
    mix_gain,
    x_weight,
    gate_weight,
    conv_taps,
    a_maps,
    i_maps,
    decay_rate,
    pace,
    jumps,
    out_gain,
    out_weight,
):
    f32 = jnp.float32
    tok_rows, col_width = tokens.shape
    channels = x_weight.shape[2]
    stream = tokens
    for layer in range(LAYERS):
        w_x, w_gate, w_out = (
            lax.all_gather(x_weight[layer], "sp", axis=0, tiled=True),
            lax.all_gather(gate_weight[layer], "sp", axis=0, tiled=True),
            lax.all_gather(out_weight[layer], "sp", axis=0, tiled=True),
        )
        w_both = jnp.concatenate([w_x, w_gate], axis=1)
        xf = stream.astype(f32)
        gain = mix_gain[layer].astype(f32)
        whole = lax.all_gather(stream, "tp", axis=1, tiled=True).astype(f32)
        normed = (
            whole * lax.rsqrt(jnp.mean(whole * whole, axis=1, keepdims=True) + EPS) * gain[None, :]
        ).astype(jnp.bfloat16)
        projected = jnp.einsum("td,dc->ct", normed, w_both, preferred_element_type=f32)
        xr = projected[:channels].astype(jnp.bfloat16)
        gr = projected[channels:].astype(jnp.bfloat16)
        rim = from_behind(xr[:, tok_rows - (WIDTH - 1) :], "sp", 1)
        padded = jnp.concatenate([rim, xr], axis=1).astype(f32)
        taps = conv_taps[layer].astype(f32)
        conv = jnp.zeros((channels, tok_rows), f32)
        for k in range(WIDTH):
            conv = conv + taps[k][:, None] * padded[:, k : k + tok_rows]
        xc = conv.astype(jnp.bfloat16)
        grouped = xc.reshape(channels // HEAD, HEAD, tok_rows)
        rgate = jax.nn.sigmoid(
            jnp.einsum("hij,hit->hjt", a_maps[layer], grouped, preferred_element_type=f32).reshape(
                channels, tok_rows
            )
        )
        igate = jax.nn.sigmoid(
            jnp.einsum("hij,hit->hjt", i_maps[layer], grouped, preferred_element_type=f32).reshape(
                channels, tok_rows
            )
        )
        log_a = -GATE_C * rgate * decay_rate[layer][:, None] * pace[None, :] + jumps[None, :]
        decay = jnp.exp(log_a)
        drive = jnp.sqrt(-jnp.expm1(2.0 * log_a)) * igate * xc.astype(f32)
        decay_run, local_state = lax.associative_scan(combine, (decay, drive), axis=1)
        identity = (jnp.ones((channels,), f32), jnp.zeros((channels,), f32))
        incoming = prefix((decay_run[:, -1], local_state[:, -1]), "sp", combine, identity)
        state = local_state + decay_run * incoming[1][:, None]
        rec = state * jax.nn.gelu(gr.astype(f32))
        mixed = (rec * out_gain[layer].astype(f32)[:, None]).astype(jnp.bfloat16)
        squares = lax.psum(jnp.sum(rec * rec, axis=0), "tp")
        out_scale = lax.rsqrt(squares / D_REC + EPS)
        update = jnp.einsum(
            "ct,cd->td",
            lax.all_gather(mixed, "tp", axis=0, tiled=True),
            w_out,
            preferred_element_type=f32,
        )
        stream = (xf + update * out_scale[:, None]).astype(jnp.bfloat16)
    return stream


def solution(mesh):
    in_specs = (
        P("sp", "tp"),
        P(),
        P(None, "sp", "tp"),
        P(None, "sp", "tp"),
        P(None, None, "tp"),
        P(None, "tp", None, None),
        P(None, "tp", None, None),
        P(None, "tp"),
        P("sp"),
        P("sp"),
        P(None, "tp"),
        P(None, "sp", "tp"),
    )
    out_specs = P("sp", "tp")
    return jax.shard_map(body, mesh=mesh, in_specs=in_specs, out_specs=out_specs, check_vma=False)
```

profile of v0, /device:TPU:24, one launch (start us, length us, event | category | flops | bytes accessed | tf_op | source)
XLA Modules:
  0.0 362.8 jit_solution(18347026842452587687)
XLA Ops:
  6.5 0.7 all-gather.21.cloned.1.call-update
  7.3 1.7 fusion.103
  9.1 1.7 fusion.104
  10.8 1.7 fusion.102
  12.6 1.4 slice_convert_fusion
  13.9 0.7 slice_convert_fusion.2
  14.6 1.3 slice_multiply_fusion.8
  16.0 1.4 slice_convert_fusion.4
  17.9 35.9 %all-gather.21.cloned.1.call-done = bf16[768,2048]{1,0:T(8,128)(2,1)} async-done(((bf16[768,512]{1,0:T(8,128)(2,1)}), bf16[768,2048]{1,0:T(8,128)(2,1)}) %all-gather.21.cloned.1.call-update) | async-done | bytes 3145744 | tf_op jit(solution)/shard_map/all_gather | solution.py:66
  53.9 2.7 fusion
  56.6 19.9 %all-gather.29.cloned.1.call-done = bf16[1,2048,256]{2,1,0:T(8,128)(2,1)} async-done(((bf16[1,256,256]{2,1,0:T(8,128)(2,1)}), bf16[1,2048,256]{2,1,0:T(8,128)(2,1)}) %all-gather.29.cloned.1.call-update) | async-done | bytes 1048592 | tf_op jit(solution)/shard_map/all_gather | solution.py:59
  76.5 23.5 %all-gather.31.cloned.1.call-done = bf16[1,2048,256]{2,1,0:T(8,128)(2,1)} async-done(((bf16[1,256,256]{2,1,0:T(8,128)(2,1)}), bf16[1,2048,256]{2,1,0:T(8,128)(2,1)}) %all-gather.31.cloned.1.call-update) | async-done | bytes 1048592 | tf_op jit(solution)/shard_map/all_gather | solution.py:60
  100.0 3.4 fusion.20
  103.4 0.9 copy-done.2
  104.2 2.1 collective-permute-start
  106.4 1.1 slice.896
  107.5 1.7 collective-permute-done
  110.9 1.2 copy.154
  112.1 2.1 convert_multiply_fusion.11
  115.7 1.5 slice.701
  117.2 1.1 multiply_add_fusion.5
  124.3 8.0 %all-gather.3 = f32[2048,1]{0,1:T(1,128)S(1)} all-gather(f32[256,1]{0,1:T(1,128)S(1)} %slice_add_fusion.4), channel_id=5, replica_groups=mesh['sp'=8,'tp'=4] {'sp'}, dimensions={0}, use_global_device_ids=true | all-gather | bytes 9216 | tf_op jit(solution)/shard_map/all_gather | solution.py:24
  133.8 10.9 %all-gather.2 = f32[2048,1]{0,1:T(1,128)S(1)} all-gather(f32[256,1]{0,1:T(1,128)S(1)} %slice_add_fusion.5), channel_id=4, replica_groups=mesh['sp'=8,'tp'=4] {'sp'}, dimensions={0}, use_global_device_ids=true | all-gather | bytes 9216 | tf_op jit(solution)/shard_map/all_gather | solution.py:24
  145.7 1.5 multiply_reduce_fusion.1
  147.2 0.8 multiply_convert_fusion.1
  148.1 9.7 %psum.14 = f32[768]{0:T(1024)S(1)} all-reduce(f32[768]{0:T(1024)S(1)} %get-tuple-element.121), channel_id=1, replica_groups=mesh['sp'=8,'tp'=4] {'tp'}, use_global_device_ids=true, to_apply=%region_4.5 | all-reduce | flops 768 | bytes 6144 | tf_op jit(solution)/shard_map/psum | solution.py:100
  157.8 21.9 %all-gather.23.cloned.1.call-done = bf16[1024,768]{0,1:T(8,128)(2,1)} async-done(((bf16[256,768]{0,1:T(8,128)(2,1)}), bf16[1024,768]{0,1:T(8,128)(2,1)}) %all-gather.23.cloned.1.call-update) | async-done | bytes 1572880 | tf_op jit(solution)/shard_map/all_gather | solution.py:104
  179.7 3.8 %add_convert_fusion.1 = bf16[768,512]{1,0:T(8,128)(2,1)} fusion(bf16[768,512]{1,0:T(8,128)(2,1)} %param.16, bf16[1024,768]{0,1:T(8,128)(2,1)} %all-gather.23.cloned.1.call-done, bf16[1,1024,512]{2,1,0:T(8,128)(2,1)} %all-gather.33.cloned.1.call-done, f32[768]{0:T(1024)S(1)} %add_rsqrt_fusion.2), kind=kOutput, calls=%fused_computation.29 | convolution fusion | flops 806879232 | bytes 4197376 | tf_op jit(solution)/shard_map/ct,cd->td/dot_general | solution.py:102
  186.1 41.4 %all-gather.25.cloned.1.call-done = bf16[768,2048]{1,0:T(8,128)(2,1)} async-done(((bf16[768,512]{1,0:T(8,128)(2,1)}), bf16[768,2048]{1,0:T(8,128)(2,1)}) %all-gather.25.cloned.1.call-update) | async-done | bytes 3145744 | tf_op jit(solution)/shard_map/all_gather | solution.py:66
  227.4 2.7 fusion.3
  230.2 19.9 %all-gather.35.cloned.1.call-done = bf16[1,2048,256]{2,1,0:T(8,128)(2,1)} async-done(((bf16[1,256,256]{2,1,0:T(8,128)(2,1)}), bf16[1,2048,256]{2,1,0:T(8,128)(2,1)}) %all-gather.35.cloned.1.call-update) | async-done | bytes 1048592 | tf_op jit(solution)/shard_map/all_gather | solution.py:59
  250.1 23.4 %all-gather.37.cloned.1.call-done = bf16[1,2048,256]{2,1,0:T(8,128)(2,1)} async-done(((bf16[1,256,256]{2,1,0:T(8,128)(2,1)}), bf16[1,2048,256]{2,1,0:T(8,128)(2,1)}) %all-gather.37.cloned.1.call-update) | async-done | bytes 1048592 | tf_op jit(solution)/shard_map/all_gather | solution.py:60
  273.5 3.4 fusion.25
  276.9 0.9 copy-done.3
  277.8 2.1 collective-permute-start.1
  280.0 1.1 slice.965
  281.0 1.7 collective-permute-done.1
  284.6 1.2 copy.160
  285.7 2.1 convert_multiply_fusion.10
  289.3 1.5 slice.809
  290.8 1.1 multiply_add_fusion.4
  297.3 8.0 %all-gather.8 = f32[2048,1]{0,1:T(1,128)S(1)} all-gather(f32[256,1]{0,1:T(1,128)S(1)} %slice_add_fusion), channel_id=10, replica_groups=mesh['sp'=8,'tp'=4] {'sp'}, dimensions={0}, use_global_device_ids=true | all-gather | bytes 9216 | tf_op jit(solution)/shard_map/all_gather | solution.py:24
  306.3 10.9 %all-gather.7 = f32[2048,1]{0,1:T(1,128)S(1)} all-gather(f32[256,1]{0,1:T(1,128)S(1)} %slice_add_fusion.1), channel_id=9, replica_groups=mesh['sp'=8,'tp'=4] {'sp'}, dimensions={0}, use_global_device_ids=true | all-gather | bytes 9216 | tf_op jit(solution)/shard_map/all_gather | solution.py:24
  318.2 1.5 multiply_reduce_fusion
  319.7 0.8 multiply_convert_fusion
  320.5 9.7 %psum.15 = f32[768]{0:T(1024)S(1)} all-reduce(f32[768]{0:T(1024)S(1)} %get-tuple-element.115), channel_id=1, replica_groups=mesh['sp'=8,'tp'=4] {'tp'}, use_global_device_ids=true, to_apply=%region_9.10 | all-reduce | flops 768 | bytes 6144 | tf_op jit(solution)/shard_map/psum | solution.py:100
  330.3 21.9 %all-gather.27.cloned.1.call-done = bf16[1024,768]{0,1:T(8,128)(2,1)} async-done(((bf16[256,768]{0,1:T(8,128)(2,1)}), bf16[1024,768]{0,1:T(8,128)(2,1)}) %all-gather.27.cloned.1.call-update) | async-done | bytes 1572880 | tf_op jit(solution)/shard_map/all_gather | solution.py:104
  352.2 3.8 %add_convert_fusion = bf16[768,512]{1,0:T(8,128)(2,1)} fusion(bf16[768,512]{1,0:T(8,128)(2,1)} %add_convert_fusion.1, bf16[1024,768]{0,1:T(8,128)(2,1)} %all-gather.27.cloned.1.call-done, bf16[1,1024,512]{2,1,0:T(8,128)(2,1)} %all-gather.39.cloned.1.call-done, f32[768]{0:T(1024)S(1)} %add_rsqrt_fusion), kind=kOutput, calls=%fused_computation.28 | convolution fusion | flops 806879232 | bytes 4197376 | tf_op jit(solution)/shard_map/ct,cd->td/dot_general | solution.py:102
  (411 shorter events, 24.1 us)
Async XLA Ops:
  6.5 47.3 %all-gather.21.cloned.1.call-start = ((), (), s32[]{:S(2)}) async-start(), calls=%async_computation | async-start | bytes 3932160 | tf_op jit(solution)/shard_map/all_gather | solution.py:66
  7.3 69.3 %all-gather.29.cloned.1.call-start = ((), (), s32[]{:S(2)}) async-start(), calls=%async_computation.4 | async-start | bytes 1179648 | tf_op jit(solution)/shard_map/all_gather | solution.py:59
  9.0 91.0 %all-gather.31.cloned.1.call-start = ((), (), s32[]{:S(2)}) async-start(), calls=%async_computation.5 | async-start | bytes 1179648 | tf_op jit(solution)/shard_map/all_gather | solution.py:60
  10.8 147.1 %all-gather.33.cloned.1.call-start = ((), (), s32[]{:S(2)}) async-start(), calls=%async_computation.6 | async-start | bytes 1179648 | tf_op jit(solution)/shard_map/all_gather | solution.py:61
  12.5 167.2 %all-gather.23.cloned.1.call-start = ((), (), s32[]{:S(2)}) async-start(), calls=%async_computation.1 | async-start | bytes 1966080 | tf_op jit(solution)/shard_map/all_gather | solution.py:104
  53.9 46.1 %copy-start = (bf16[768,2048]{1,0:T(8,128)(2,1)S(1)}, bf16[768,2048]{1,0:T(8,128)(2,1)}, u32[]{:S(2)}) copy-start(bf16[768,2048]{1,0:T(8,128)(2,1)} %all-gather.21.cloned.1.call-done) | copy-start | bytes 9437188
  103.4 0.9 copy-start.2
  104.2 4.9 %collective-permute-start = (bf16[256,3]{0,1:T(4,128)(2,1)S(1)}, bf16[256,3]{0,1:T(4,128)(2,1)S(1)}, u32[]{:S(2)}, u32[]{:S(2)}) collective-permute-start(bf16[256,3]{0,1:T(4,128)(2,1)S(1)} %slice.895), channel_id=1, source_target_pairs={{0,4},{4,8},{8,12},{12,16},{16,20},{20,24},{24,28},{1,5},{5,9},{9,... | collective-permute-start | bytes 4616 | tf_op jit(solution)/shard_map/ppermute | solution.py:19
  106.4 3.4 copy-start.15
  109.6 0.9 copy-start.17
  110.2 1.9 copy-start.4
  110.2 1.9 copy-start.5
  124.0 9.5 %copy-start.11 = (f32[256,1]{0,1:T(1,128)S(1)}, f32[256,1]{0,1:T(1,128)}, u32[]{:S(2)}) copy-start(f32[256,1]{0,1:T(1,128)} %slice.933) | copy-start | bytes 3076
  133.8 13.4 %copy-start.14 = (f32[1,256]{1,0:T(1,128)S(1)}, f32[1,256]{1,0:T(1,128)}, u32[]{:S(2)}) copy-start(f32[1,256]{1,0:T(1,128)} %get-tuple-element.228) | copy-start | bytes 3076
  148.0 79.4 %all-gather.25.cloned.1.call-start = ((), (), s32[]{:S(2)}) async-start(), calls=%async_computation.2 | async-start | bytes 3932160 | tf_op jit(solution)/shard_map/all_gather | solution.py:66
  183.6 89.9 %copy-start.10 = (f32[1,2048]{1,0:T(1,128)S(1)}, f32[1,2048]{1,0:T(1,128)}, u32[]{:S(2)}) copy-start(f32[1,2048]{1,0:T(1,128)} %get-tuple-element.193) | copy-start | bytes 24580
  183.6 66.5 %all-gather.35.cloned.1.call-start = ((), (), s32[]{:S(2)}) async-start(), calls=%async_computation.7 | async-start | bytes 1179648 | tf_op jit(solution)/shard_map/all_gather | solution.py:59
  184.3 89.1 %all-gather.37.cloned.1.call-start = ((), (), s32[]{:S(2)}) async-start(), calls=%async_computation.8 | async-start | bytes 1179648 | tf_op jit(solution)/shard_map/all_gather | solution.py:60
  185.1 145.2 %all-gather.39.cloned.1.call-start = ((), (), s32[]{:S(2)}) async-start(), calls=%async_computation.9 | async-start | bytes 1179648 | tf_op jit(solution)/shard_map/all_gather | solution.py:61
  185.8 166.4 %all-gather.27.cloned.1.call-start = ((), (), s32[]{:S(2)}) async-start(), calls=%async_computation.3 | async-start | bytes 1966080 | tf_op jit(solution)/shard_map/all_gather | solution.py:104
  227.4 46.0 %copy-start.1 = (bf16[768,2048]{1,0:T(8,128)(2,1)S(1)}, bf16[768,2048]{1,0:T(8,128)(2,1)}, u32[]{:S(2)}) copy-start(bf16[768,2048]{1,0:T(8,128)(2,1)} %all-gather.25.cloned.1.call-done) | copy-start | bytes 9437188
  273.5 9.3 %copy-start.6 = (f32[1,1,256]{2,1,0:T(1,128)S(1)}, f32[1,1,256]{2,1,0:T(1,128)}, u32[]{:S(2)}) copy-start(f32[1,1,256]{2,1,0:T(1,128)} %get-tuple-element.205) | copy-start | bytes 3076
  273.5 9.3 %copy-start.7 = (f32[1,1,256]{2,1,0:T(1,128)S(1)}, f32[1,1,256]{2,1,0:T(1,128)}, u32[]{:S(2)}) copy-start(f32[1,1,256]{2,1,0:T(1,128)} %get-tuple-element.206) | copy-start | bytes 3076
  273.5 9.3 %copy-start.8 = (f32[1,1,256]{2,1,0:T(1,128)S(1)}, f32[1,1,256]{2,1,0:T(1,128)}, u32[]{:S(2)}) copy-start(f32[1,1,256]{2,1,0:T(1,128)} %get-tuple-element.207) | copy-start | bytes 3076
  273.5 9.3 %copy-start.9 = (f32[1,1,256]{2,1,0:T(1,128)S(1)}, f32[1,1,256]{2,1,0:T(1,128)}, u32[]{:S(2)}) copy-start(f32[1,1,256]{2,1,0:T(1,128)} %get-tuple-element.208) | copy-start | bytes 3076
  276.9 0.9 copy-start.3
  277.8 4.9 %collective-permute-start.1 = (bf16[256,3]{0,1:T(4,128)(2,1)S(1)}, bf16[256,3]{0,1:T(4,128)(2,1)S(1)}, u32[]{:S(2)}, u32[]{:S(2)}) collective-permute-start(bf16[256,3]{0,1:T(4,128)(2,1)S(1)} %slice.964), channel_id=1, source_target_pairs={{0,4},{4,8},{8,12},{12,16},{16,20},{20,24},{24,28},{1,5},{5,9},{9,... | collective-permute-start | bytes 4616 | tf_op jit(solution)/shard_map/ppermute | solution.py:19
  280.0 3.4 copy-start.16
  282.9 1.0 copy-start.18
  283.8 1.9 copy-start.12
  306.1 13.5 %copy-start.13 = (f32[1,256]{1,0:T(1,128)S(1)}, f32[1,256]{1,0:T(1,128)}, u32[]{:S(2)}) copy-start(f32[1,256]{1,0:T(1,128)} %get-tuple-element.227) | copy-start | bytes 3076
Sparse Core Ops, SparseCore 0:
  9.2 44.6 all-gather.20
  55.5 20.9 all-gather.28
  78.1 21.8 all-gather.30
  101.4 21.8 all-gather.32
  148.2 31.5 all-gather.22
  183.7 43.6 all-gather.24
  229.0 20.9 all-gather.34
  251.7 21.7 all-gather.36
  275.1 21.8 all-gather.38
  320.7 31.5 all-gather.26
where the time goes:
time: 365 us; the launch traced here: 363 us
  waiting for transfers between devices  214 us (59%)
  blocking collectives  57.1 us (16%)
  local copies, waits for them, and re-layouts  27.7 us (8%)
  other arithmetic  27 us (7%)
  matrix products  16.1 us (4%)
  between operations  15.8 us (4%)
  starting transfers between devices  4.79 us (1%)
    all_gather x2, waiting for transfers between devices, body(): whole = lax.all_gather(stream, 'tp', axis=1, tiled=True).astype(f32)  77.3 us
    all_gather x2, waiting for transfers between devices, body(): lax.all_gather(gate_weight[layer], 'sp', axis=0, tiled=True)  46.9 us
    all_gather x2, waiting for transfers between devices, body(): lax.all_gather(mixed, 'tp', axis=0, tiled=True)  43.8 us
    all_gather x2, waiting for transfers between devices, body(): lax.all_gather(x_weight[layer], 'sp', axis=0, tiled=True)  39.8 us
    all_gather x4, blocking collectives, prefix(): gathered = jax.tree.map(lambda a: lax.all_gather(a, axis), part)  37.7 us
    psum x2, blocking collectives, body(): squares = lax.psum(jnp.sum(rec * rec, axis=0), 'tp')  19.4 us
    slice x128, local copies, waits for them, and re-layouts, body(): lax.associative_scan(combine, (decay, drive), axis=1)  12.2 us
    dot_general x2, matrix products, body(): jnp.einsum('ct,cd->td', lax.all_gather(mixed, 'tp', axis=0, tiled=True),...  7.63 us
  transfers between devices with their start and end apart: 12, of which 10 were waited for; matrix products, arithmetic and copies ran while one was open for 17% of the time, Pallas kernels for 0%

commit v1 on v0

v1 whole, which is shorter than its diff:
```python
import functools

import jax
import jax.numpy as jnp
from jax import lax
from jax.experimental import pallas as pl
from jax.experimental.pallas import tpu as pltpu
from jax.sharding import PartitionSpec as P

EPS = 1e-06
GATE_C = 8.0
WIDTH = 4
PAD = 8
SEGS = 8
F32 = jnp.float32
BF16 = jnp.bfloat16


def one_minus_exp(y):
    p = 1.0 / 5040.0
    for d in (720.0, 120.0, 24.0, 6.0, 2.0, 1.0):
        p = p * y + 1.0 / d
    return jnp.where(y > -0.35, -y * p, 1.0 - jnp.exp(y))


def kernel(
    dims,
    tokens, gain, xw, gw, taps, am, im, rate, pj, og, ow,
    out,
    xs, mx, wx, wg, wo, bda, bdi, xp, gl, a_s, b_s, ea_s, eb_s, tot, st, ogf,
    sem_send, sem_recv, w_send, w_fsend, w_recv, w_part, own_sem, tok_sem,
    rim_sem, st_send, st_recv, og_send, og_recv,
):
    n_sp, n_tp, layers, chunks = dims
    me = lax.axis_index("sp")
    my = lax.axis_index("tp")
    tok_rows, cols = tokens.shape
    ch = xw.shape[2]
    t_rows = tok_rows // chunks
    seg = t_rows // SEGS
    relay = n_tp == 4
    n_z = n_sp // 2
    z, k = me // 2, me % 2
    partner = 2 * z + 1 - k

    def dev(sp=None, tp=None):
        return {"sp": me if sp is None else sp, "tp": my if tp is None else tp}

    barrier = pltpu.get_barrier_semaphore()
    for d in range(1, n_sp):
        pl.semaphore_signal(barrier, inc=1, device_id=dev(sp=(me + d) % n_sp))
    for d in range(1, n_tp):
        pl.semaphore_signal(barrier, inc=1, device_id=dev(tp=(my + d) % n_tp))
    pl.semaphore_wait(barrier, n_sp + n_tp - 2)

    if relay:
        xb, yb = my % 2, my // 2
        xn = yb * 2 + (1 - xb)
        yn = (1 - yb) * 2 + xb
        direct = [(0, xn), (1, yn)]
        senders = [xn, yn]
        far = 3 - my
    else:
        direct = [(d, (my + d) % n_tp) for d in range(1, n_tp)]
        senders = [(my + d) % n_tp for d in range(1, n_tp)]
        far = None
    bufs = (xs, mx)

    def rows(c):
        return pl.ds(pl.multiple_of(c * t_rows, t_rows), t_rows)

    def own_copies(kind, l, c):
        buf = bufs[kind]
        place = buf.at[l, my, rows(c)]
        src = tokens.at[rows(c)] if (kind == 0 and l == 0) else place
        return [
            pltpu.make_async_remote_copy(
                src_ref=src, dst_ref=place,
                send_sem=sem_send.at[kind, l, c, slot], recv_sem=sem_recv.at[kind, l, c, my],
                device_id=dev(tp=peer),
            )
            for slot, peer in direct
        ]

    def send_own(kind, l, c):
        for copy in own_copies(kind, l, c):
            copy.start()

    def arrived(kind, l, c, src):
        place = bufs[kind].at[l, src, rows(c)]
        pltpu.make_async_copy(place, place, sem_recv.at[kind, l, c, src]).wait()

    def fwd_copy(kind, l, c):
        par = c % 2
        src = xn * (1 - par) + yn * par
        dst = yn * (1 - par) + xn * par
        place = bufs[kind].at[l, src, rows(c)]
        return pltpu.make_async_remote_copy(
            src_ref=place, dst_ref=place,
            send_sem=sem_send.at[kind, l, c, 2], recv_sem=sem_recv.at[kind, l, c, src],
            device_id=dev(tp=dst),
        )

    def near(kind, l, c):
        for s in senders:
            arrived(kind, l, c, s)
        if relay:
            fwd_copy(kind, l, c).start()

    def farther(kind, l, c):
        if relay:
            arrived(kind, l, c, far)

    w_args = (xw, gw, ow)
    w_bufs = (wx, wg, wo)

    def w_block(i, l, who):
        blk = w_args[i].shape[1]
        return w_bufs[i].at[l, pl.ds(pl.multiple_of(who * blk, blk), blk)]

    def w_copies(i, l):
        place = w_block(i, l, me)
        res = [
            pltpu.make_async_remote_copy(
                src_ref=w_args[i].at[l], dst_ref=place,
                send_sem=w_send.at[i, l], recv_sem=w_recv.at[i, l],
                device_id=dev(sp=((z + d) % n_z) * 2 + k),
            )
            for d in range(1, n_z)
        ]
        res.append(
            pltpu.make_async_remote_copy(
                src_ref=w_args[i].at[l], dst_ref=place,
                send_sem=w_send.at[i, l], recv_sem=w_part.at[i, l],
                device_id=dev(sp=partner),
            )
        )
        return res

    def w_own(i, l):
        return pltpu.make_async_copy(w_args[i].at[l], w_block(i, l, me), own_sem.at[i, l])

    def w_wait(i, l, sem, count):
        blk = w_args[i].shape[1]
        part = w_bufs[i].at[l, pl.ds(0, count * blk)]
        pltpu.make_async_copy(part, part, sem).wait()

    def w_forward(i, l):
        w_wait(i, l, w_recv.at[i, l], n_z - 1)
        for d in range(1, n_z):
            who = ((z + d) % n_z) * 2 + k
            pltpu.make_async_remote_copy(
                src_ref=w_block(i, l, who), dst_ref=w_block(i, l, who),
                send_sem=w_fsend.at[i, l], recv_sem=w_part.at[i, l],
                device_id=dev(sp=partner),
            ).start()

    def w_ready(i, l):
        w_wait(i, l, w_part.at[i, l], n_z)
        w_own(i, l).wait()

    tok_copy = pltpu.make_async_copy(tokens, xs.at[0, my], tok_sem)
    for c in range(chunks - 1, max(chunks - 3, -1), -1):
        send_own(0, 0, c)
    tok_copy.start()
    for l in range(layers):
        for i in range(3):
            for copy in w_copies(i, l):
                copy.start()
            w_own(i, l).start()

    row8 = lax.broadcasted_iota(jnp.int32, (8, ch), 0)
    ogv = og[...].astype(F32)
    acc = jnp.zeros((8, ch), F32)
    for l in range(layers):
        acc = jnp.where(row8 == l, ogv[l : l + 1], acc)
    ogf[my] = acc
    og_copies = [
        pltpu.make_async_remote_copy(
            src_ref=ogf.at[my], dst_ref=ogf.at[my],
            send_sem=og_send.at[d], recv_sem=og_recv.at[my],
            device_id=dev(tp=(my + d) % n_tp),
        )
        for d in range(1, n_tp)
    ]
    for copy in og_copies:
        copy.start()
    heads, head = am.shape[1], am.shape[2]
    for l in range(layers):
        for src, dst in ((am, bda), (im, bdi)):
            for h in range(heads):
                m = src[l, h].astype(F32)
                parts = [m if j == h else jnp.zeros((head, head), F32) for j in range(heads)]
                line = jnp.concatenate(parts, axis=1) if heads > 1 else m
                dst[l, h * head : (h + 1) * head, :] = line.astype(BF16)
    for l in range(layers):
        @pl.when(me == 0)
        def _():
            xp[l, 0:PAD, :] = jnp.zeros((PAD, ch), F32)

    def rim_copy(l):
        return pltpu.make_async_remote_copy(
            src_ref=xp.at[l, pl.ds(tok_rows, PAD)], dst_ref=xp.at[l, pl.ds(0, PAD)],
            send_sem=rim_sem.at[l, 0], recv_sem=rim_sem.at[l, 1],
            device_id=dev(sp=(me + 1) % n_sp),
        )

    def project(l, c):
        r = rows(c)
        total = jnp.zeros((t_rows, 1), F32)
        for p in range(n_tp):
            v = xs[l, p, r, :].astype(F32)
            total = total + jnp.sum(v * v, axis=1, keepdims=True)
        rs = lax.rsqrt(total / (n_tp * cols) + EPS)
        xr = jnp.zeros((t_rows, ch), F32)
        gr = jnp.zeros((t_rows, ch), F32)
        for p in range(n_tp):
            v = xs[l, p, r, :].astype(F32)
            g = gain[l : l + 1, p * cols : (p + 1) * cols].astype(F32)
            nv = (v * rs * g).astype(BF16)
            xr += jnp.dot(nv, wx[l, p * cols : (p + 1) * cols, :], preferred_element_type=F32)
            gr += jnp.dot(nv, wg[l, p * cols : (p + 1) * cols, :], preferred_element_type=F32)
        xp[l, pl.ds(pl.multiple_of(c * t_rows + PAD, 8), t_rows), :] = xr.astype(BF16).astype(F32)
        gl[c] = jax.nn.gelu(gr.astype(BF16).astype(F32))

    def gates(l, c):
        blk = xp[l, pl.ds(pl.multiple_of(c * t_rows, 8), t_rows + PAD), :]
        conv = jnp.zeros((t_rows, ch), F32)
        for j in range(WIDTH):
            o = PAD - (WIDTH - 1) + j
            conv = conv + taps[l, j : j + 1, :].astype(F32) * blk[o : o + t_rows]
        xc = conv.astype(BF16)
        rg = jax.nn.sigmoid(jnp.dot(xc, bda[l], preferred_element_type=F32))
        ig = jax.nn.sigmoid(jnp.dot(xc, bdi[l], preferred_element_type=F32))
        pv = pj[rows(c), :]
        log_a = (-GATE_C * rate[l : l + 1, :]) * rg * pv[:, 0:1] + pv[:, 1:2]
        av = jnp.exp(log_a)
        bv = jnp.sqrt(one_minus_exp(2.0 * log_a)) * ig * xc.astype(F32)
        lw = a_s.shape[3]
        for q in range(a_s.shape[1]):
            a_s[c, q] = av[:, q * lw : (q + 1) * lw]
            b_s[c, q] = bv[:, q * lw : (q + 1) * lw]
            pa = jnp.ones((SEGS, lw), F32)
            hb = jnp.zeros((SEGS, lw), F32)
            for j in range(seg):
                at = pl.ds(j, SEGS, stride=seg)
                x = a_s[c, q, at, :]
                hb = x * hb + b_s[c, q, at, :]
                pa = x * pa
                a_s[c, q, at, :] = pa
                b_s[c, q, at, :] = hb
            ea = jnp.ones((1, lw), F32)
            eb = jnp.zeros((1, lw), F32)
            for s in range(SEGS):
                ea_s[c, q, s : s + 1, :] = ea
                eb_s[c, q, s : s + 1, :] = eb
                eb = pa[s : s + 1] * eb + hb[s : s + 1]
                ea = pa[s : s + 1] * ea
            tot[c, 0:1, q * lw : (q + 1) * lw] = ea
            tot[c, 1:2, q * lw : (q + 1) * lw] = eb

    def st_copy(l, to):
        return pltpu.make_async_remote_copy(
            src_ref=st.at[l, me], dst_ref=st.at[l, me],
            send_sem=st_send.at[l, to], recv_sem=st_recv.at[l, me],
            device_id=dev(sp=to),
        )

    def mix(l, c, inc):
        lw = a_s.shape[3]
        halves = []
        for q in range(a_s.shape[1]):
            part = inc[:, q * lw : (q + 1) * lw]
            lines = []
            for s in range(SEGS):
                entry = eb_s[c, q, s : s + 1, :] + ea_s[c, q, s : s + 1, :] * part
                at = slice(s * seg, (s + 1) * seg)
                lines.append(b_s[c, q, at, :] + a_s[c, q, at, :] * entry)
            halves.append(jnp.concatenate(lines, axis=0))
        state = jnp.concatenate(halves, axis=1) if len(halves) > 1 else halves[0]
        rec = state * gl[c]
        mx[l, my, rows(c), :] = (rec * og[l : l + 1, :].astype(F32)).astype(BF16)

    def update(l, c):
        r = rows(c)
        total = jnp.zeros((t_rows, 1), F32)
        acc = jnp.zeros((t_rows, cols), F32)
        for p in range(n_tp):
            m = mx[l, p, r, :]
            v = m.astype(F32) * (1.0 / ogf[p, l : l + 1, :])
            total = total + jnp.sum(v * v, axis=1, keepdims=True)
            acc += jnp.dot(m, wo[l, p * ch : (p + 1) * ch, :], preferred_element_type=F32)
        scale = lax.rsqrt(total / (n_tp * ch) + EPS)
        new = (xs[l, my, r, :].astype(F32) + acc * scale).astype(BF16)
        if l == layers - 1:
            out[r, :] = new
        else:
            xs[l + 1, my, r, :] = new
            send_own(0, l + 1, c)

    tok_copy.wait()
    for l in range(layers):
        def front(i, carry):
            c = chunks - 1 - i

            @pl.when(i < chunks)
            def _():
                near(0, l, c)
                if l == 0:
                    @pl.when(c >= 2)
                    def _():
                        send_own(0, 0, c - 2)

            @pl.when(i == 1)
            def _():
                w_forward(0, l)
                w_forward(1, l)
                w_ready(0, l)
                w_ready(1, l)

            @pl.when(i >= 1)
            def _():
                farther(0, l, c + 1)
                project(l, c + 1)

            @pl.when((i == 1) & (me < n_sp - 1))
            def _():
                rim_copy(l).start()

            @pl.when(i >= 2)
            def _():
                gates(l, c + 2)

            return carry

        lax.fori_loop(0, chunks + 1, front, 0)

        @pl.when(me > 0)
        def _():
            rim_copy(l).wait_recv()

        gates(l, 0)

        ta, tb = jnp.ones((1, ch), F32), jnp.zeros((1, ch), F32)
        for c in range(chunks):
            tb = tot[c, 0:1, :] * tb + tot[c, 1:2, :]
            ta = tot[c, 0:1, :] * ta
        st[l, me] = jnp.where(row8 == 0, ta, tb)

        def send_st(to, carry):
            st_copy(l, to).start()
            return carry

        lax.fori_loop(me + 1, n_sp, send_st, 0)
        w_forward(2, l)

        def take_st(src, inc):
            place = st.at[l, src]
            pltpu.make_async_copy(place, place, st_recv.at[l, src]).wait()
            return st[l, src, 0:1, :] * inc + st[l, src, 1:2, :]

        inc = lax.fori_loop(0, me, take_st, jnp.zeros((1, ch), F32))
        incs = []
        for c in range(chunks):
            incs.append(inc)
            inc = tot[c, 0:1, :] * inc + tot[c, 1:2, :]
        for c in range(chunks - 1, -1, -1):
            mix(l, c, incs[c])
            if c >= chunks - 2:
                send_own(1, l, c)
        w_ready(2, l)
        if l == 0:
            for d in range(1, n_tp):
                src = (my + d) % n_tp
                pltpu.make_async_copy(ogf.at[src], ogf.at[src], og_recv.at[src]).wait()

        def back(i, carry):
            c = chunks - 1 - i

            @pl.when(i < chunks)
            def _():
                near(1, l, c)

                @pl.when(c >= 2)
                def _():
                    send_own(1, l, c - 2)

            @pl.when(i >= 1)
            def _():
                farther(1, l, c + 1)
                update(l, c + 1)

            return carry

        lax.fori_loop(0, chunks + 1, back, 0)

    def drain(c, carry):
        for kind in range(2):
            for l in range(layers):
                for copy in own_copies(kind, l, c):
                    copy.wait_send()
                if relay:
                    fwd_copy(kind, l, c).wait_send()
        return carry

    lax.fori_loop(0, chunks, drain, 0)
    for l in range(layers):
        for i in range(3):
            w_wait(i, l, w_send.at[i, l], n_z)
            w_wait(i, l, w_fsend.at[i, l], n_z - 1)

        @pl.when(me < n_sp - 1)
        def _():
            rim_copy(l).wait_send()

        def st_done(to, carry):
            st_copy(l, to).wait_send()
            return carry

        lax.fori_loop(me + 1, n_sp, st_done, 0)
    for copy in og_copies:
        copy.wait_send()


def body(n_sp, n_tp, tokens, mix_gain, x_weight, gate_weight, conv_taps, a_maps, i_maps,
         decay_rate, pace, jumps, out_gain, out_weight):
    layers = x_weight.shape[0]
    tok_rows, cols = tokens.shape
    ch = x_weight.shape[2]
    d = n_tp * cols
    d_rec = n_tp * ch
    chunks = 4
    t_rows = tok_rows // chunks
    lw = min(ch, 128)
    nq = ch // lw
    pj = jnp.stack([pace, jumps], axis=1)
    vm = pl.BlockSpec(memory_space=pltpu.VMEM)
    hb = pl.BlockSpec(memory_space=pl.ANY)
    dma = pltpu.SemaphoreType.DMA
    return pl.pallas_call(
        functools.partial(kernel, (n_sp, n_tp, layers, chunks)),
        out_shape=jax.ShapeDtypeStruct((tok_rows, cols), BF16),
        in_specs=[hb, vm, hb, hb, vm, vm, vm, vm, vm, vm, hb],
        out_specs=vm,
        scratch_shapes=[
            pltpu.VMEM((layers, n_tp, tok_rows, cols), BF16),
            pltpu.VMEM((layers, n_tp, tok_rows, ch), BF16),
            pltpu.VMEM((layers, d, ch), BF16),
            pltpu.VMEM((layers, d, ch), BF16),
            pltpu.VMEM((layers, d_rec, cols), BF16),
            pltpu.VMEM((layers, ch, ch), BF16),
            pltpu.VMEM((layers, ch, ch), BF16),
            pltpu.VMEM((layers, PAD + tok_rows, ch), F32),
            pltpu.VMEM((chunks, t_rows, ch), F32),
            pltpu.VMEM((chunks, nq, t_rows, lw), F32),
            pltpu.VMEM((chunks, nq, t_rows, lw), F32),
            pltpu.VMEM((chunks, nq, SEGS, lw), F32),
            pltpu.VMEM((chunks, nq, SEGS, lw), F32),
            pltpu.VMEM((chunks, 8, ch), F32),
            pltpu.VMEM((layers, n_sp, 8, ch), F32),
            pltpu.VMEM((n_tp, 8, ch), F32),
            dma((2, layers, chunks, n_tp)),
            dma((2, layers, chunks, n_tp)),
            dma((3, layers)),
            dma((3, layers)),
            dma((3, layers)),
            dma((3, layers)),
            dma((3, layers)),
            dma,
            dma((layers, 2)),
            dma((layers, n_sp)),
            dma((layers, n_sp)),
            dma((n_tp,)),
            dma((n_tp,)),
        ],
        compiler_params=pltpu.CompilerParams(
            collective_id=0, has_side_effects=True, vmem_limit_bytes=60 * 1024 * 1024
        ),
    )(tokens, mix_gain, x_weight, gate_weight, conv_taps, a_maps, i_maps, decay_rate, pj,
      out_gain, out_weight)


def solution(mesh):
    in_specs = (
        P("sp", "tp"),
        P(),
        P(None, "sp", "tp"),
        P(None, "sp", "tp"),
        P(None, None, "tp"),
        P(None, "tp", None, None),
        P(None, "tp", None, None),
        P(None, "tp"),
        P("sp"),
        P("sp"),
        P(None, "tp"),
        P(None, "sp", "tp"),
    )
    out_specs = P("sp", "tp")
    return jax.shard_map(
        functools.partial(body, mesh.shape["sp"], mesh.shape["tp"]),
        mesh=mesh, in_specs=in_specs, out_specs=out_specs, check_vma=False,
    )
```

time: 365 us -> 148 us (0.41)
  waiting for transfers between devices: 214 us -> 0 us
  Pallas kernels: 0 us -> 144 us
  blocking collectives: 57.1 us -> 0 us
  other arithmetic: 27 us -> 0.01 us
  local copies, waits for them, and re-layouts: 27.7 us -> 3.71 us
  matrix products: 16.1 us -> 0 us
  between operations: 15.8 us -> 0.02 us
  starting transfers between devices: 4.79 us -> 0 us
    all_gather x10 -> x0, waiting for transfers between devices: 208 us -> none  [the longest x2 77.3 us: body(): whole = lax.all_gather(stream, 'tp', axis=1, tiled=True).astype(f32)]
    pallas_call x0 -> x1, Pallas kernels: none -> 144 us  [body(): pl.pallas_call(functools.partial(kernel, (n_sp, n_tp, layers, chunks)), o...]
    all_gather x4 -> x0, blocking collectives: 37.7 us -> none  [prefix(): gathered = jax.tree.map(lambda a: lax.all_gather(a, axis), part)]
    slice x136 -> x0, local copies, waits for them, and re-layouts: 20 us -> none  [the longest x128 12.2 us: body(): lax.associative_scan(combine, (decay, drive), axis=1)]
    psum x2 -> x0, blocking collectives: 19.4 us -> none  [body(): squares = lax.psum(jnp.sum(rec * rec, axis=0), 'tp')]
    dot_general x8 -> x0, matrix products: 16.1 us -> none  [the longest x2 7.63 us: body(): jnp.einsum('ct,cd->td', lax.all_gather(mixed, 'tp', axis=0, tiled=True),...]
    reduce_sum x4 -> x0, other arithmetic: 8.45 us -> none  [the longest x2 5.44 us: body(): jnp.mean(whole * whole, axis=1, keepdims=True) + EPS]
    mul x4 -> x0, other arithmetic: 6.98 us -> none  [the longest x2 4.26 us: body(): drive = jnp.sqrt(-jnp.expm1(2.0 * log_a)) * igate * xc.astype(f32)]
  transfers between devices with their start and end apart: 12 -> 0, of which waited for: 10 -> 0; matrix products, arithmetic and copies ran while one was open for 17% -> 0% of each run, Pallas kernels for 0% -> 0%
where the time goes in v1:
time: 148 us
  Pallas kernels  144 us (97%)
  local copies, waits for them, and re-layouts  3.71 us (3%)
    pallas_call x1, Pallas kernels, body(): pl.pallas_call(functools.partial(kernel, (n_sp, n_tp, layers, chunks)), o...  144 us

profile of v1, /device:TPU:24, one launch (start us, length us, event | category | flops | bytes accessed | tf_op | source)
XLA Modules:
  0.0 147.8 jit_solution(7858641003389779151)
XLA Ops:
  0.0 0.0 copy-start
  0.0 0.7 stack.9
  0.7 0.0 copy-done
  0.7 0.9 copy.15.pj
  1.7 144.1 %shard_map.118 = bf16[768,512]{1,0:T(8,128)(2,1)} custom-call(bf16[768,512]{1,0:T(8,128)(2,1)} %tokens.1, bf16[2,2048]{1,0:T(2,128)(2,1)} %gain.1, bf16[2,256,256]{2,1,0:T(8,128)(2,1)} %xw.1, bf16[2,256,256]{2,1,0:T(8,128)(2,1)} %gw.1, bf16[2,4,256]{2,1,0:T(4,128)(2,1)} %taps.1, bf16[2,4,64,64]{3,2,1,0:T(8,128)(2,1)} %am.1, bf16[2,4,64,64]{3,2,1,0:T(8,128)(2,1)} %im.1, ...), custom_call_target="tpu_custom_call" | custom-call | tf_op jit(solution)/shard_map/pallas_call | solution.py:440
  145.7 2.1 %copy.17 = bf16[768,512]{1,0:T(8,128)(2,1)} copy(bf16[768,512]{1,0:T(8,128)(2,1)} %shard_map.118) | data formatting | bytes 1572864
  (2 shorter events, 0.0 us)
Async XLA Ops:
  0.0 0.7 copy-start

commit v2 on v1

--- a/solution.py
+++ b/solution.py
@@ -90,22 +90,27 @@
         place = bufs[kind].at[l, src, rows(c)]
         pltpu.make_async_copy(place, place, sem_recv.at[kind, l, c, src]).wait()
 
-    def fwd_copy(kind, l, c):
-        par = c % 2
-        src = xn * (1 - par) + yn * par
-        dst = yn * (1 - par) + xn * par
-        place = bufs[kind].at[l, src, rows(c)]
-        return pltpu.make_async_remote_copy(
-            src_ref=place, dst_ref=place,
-            send_sem=sem_send.at[kind, l, c, 2], recv_sem=sem_recv.at[kind, l, c, src],
-            device_id=dev(tp=dst),
-        )
+    def fwd_copies(kind, l, c):
+        half = t_rows // 2
+        res = []
+        for n, (src, dst) in enumerate(((xn, yn), (yn, xn))):
+            at = pl.ds(pl.multiple_of(c * t_rows + n * half, half), half)
+            place = bufs[kind].at[l, src, at]
+            res.append(
+                pltpu.make_async_remote_copy(
+                    src_ref=place, dst_ref=place,
+                    send_sem=sem_send.at[kind, l, c, 2 + n], recv_sem=sem_recv.at[kind, l, c, src],
+                    device_id=dev(tp=dst),
+                )
+            )
+        return res
 
     def near(kind, l, c):
         for s in senders:
             arrived(kind, l, c, s)
         if relay:
-            fwd_copy(kind, l, c).start()
+            for copy in fwd_copies(kind, l, c):
+                copy.start()
 
     def farther(kind, l, c):
         if relay:
@@ -137,6 +142,10 @@
         )
         return res
 
+    def w_issue(i, l):
+        for copy in w_copies(i, l):
+            copy.start()
+
     def w_own(i, l):
         return pltpu.make_async_copy(w_args[i].at[l], w_block(i, l, me), own_sem.at[i, l])
 
@@ -163,10 +172,10 @@
     for c in range(chunks - 1, max(chunks - 3, -1), -1):
         send_own(0, 0, c)
     tok_copy.start()
+    w_issue(0, 0)
+    w_issue(1, 0)
     for l in range(layers):
         for i in range(3):
-            for copy in w_copies(i, l):
-                copy.start()
             w_own(i, l).start()
 
     row8 = lax.broadcasted_iota(jnp.int32, (8, ch), 0)
@@ -315,6 +324,7 @@
             def _():
                 w_forward(0, l)
                 w_forward(1, l)
+                w_issue(2, l)
                 w_ready(0, l)
                 w_ready(1, l)
 
@@ -353,6 +363,9 @@
 
         lax.fori_loop(me + 1, n_sp, send_st, 0)
         w_forward(2, l)
+        if l + 1 < layers:
+            w_issue(0, l + 1)
+            w_issue(1, l + 1)
 
         def take_st(src, inc):
             place = st.at[l, src]
@@ -400,7 +413,8 @@
                 for copy in own_copies(kind, l, c):
                     copy.wait_send()
                 if relay:
-                    fwd_copy(kind, l, c).wait_send()
+                    for copy in fwd_copies(kind, l, c):
+                        copy.wait_send()
         return carry
 
     lax.fori_loop(0, chunks, drain, 0)

time: 148 us -> 117 us (0.79)
  Pallas kernels: 144 us -> 113 us
    pallas_call x1, Pallas kernels: 144 us -> 113 us  [body(): pl.pallas_call(functools.partial(kernel, (n_sp, n_tp, layers, chunks)), o...]
where the time goes in v2:
time: 117 us; the launch traced here: 116 us
  Pallas kernels  113 us (97%)
  local copies, waits for them, and re-layouts  3.71 us (3%)
    pallas_call x1, Pallas kernels, body(): pl.pallas_call(functools.partial(kernel, (n_sp, n_tp, layers, chunks)), o...  113 us

profile of v2, /device:TPU:24, one launch (start us, length us, event | category | flops | bytes accessed | tf_op | source)
XLA Modules:
  0.0 116.4 jit_solution(16285793936610884615)
XLA Ops:
  0.0 0.0 copy-start
  0.0 0.7 stack.9
  0.7 0.0 copy-done
  0.7 0.9 copy.15.pj
  1.7 112.6 %shard_map.118 = bf16[768,512]{1,0:T(8,128)(2,1)} custom-call(bf16[768,512]{1,0:T(8,128)(2,1)} %tokens.1, bf16[2,2048]{1,0:T(2,128)(2,1)} %gain.1, bf16[2,256,256]{2,1,0:T(8,128)(2,1)} %xw.1, bf16[2,256,256]{2,1,0:T(8,128)(2,1)} %gw.1, bf16[2,4,256]{2,1,0:T(4,128)(2,1)} %taps.1, bf16[2,4,64,64]{3,2,1,0:T(8,128)(2,1)} %am.1, bf16[2,4,64,64]{3,2,1,0:T(8,128)(2,1)} %im.1, ...), custom_call_target="tpu_custom_call" | custom-call | tf_op jit(solution)/shard_map/pallas_call | solution.py:454
  114.3 2.1 %copy.17 = bf16[768,512]{1,0:T(8,128)(2,1)} copy(bf16[768,512]{1,0:T(8,128)(2,1)} %shard_map.118) | data formatting | bytes 1572864
  (2 shorter events, 0.0 us)
Async XLA Ops:
  0.0 0.7 copy-start

commit v3 on v2

--- a/solution.py
+++ b/solution.py
@@ -27,7 +27,7 @@
     dims,
     tokens, gain, xw, gw, taps, am, im, rate, pj, og, ow,
     out,
-    xs, mx, wx, wg, wo, bda, bdi, xp, gl, a_s, b_s, ea_s, eb_s, tot, st, ogf,
+    nrm, xs, mx, wx, wg, wo, bda, bdi, xp, gl, a_s, b_s, ea_s, eb_s, tot, st, ogf,
     sem_send, sem_recv, w_send, w_fsend, w_recv, w_part, own_sem, tok_sem,
     rim_sem, st_send, st_recv, og_send, og_recv,
 ):
@@ -131,7 +131,7 @@
                 send_sem=w_send.at[i, l], recv_sem=w_recv.at[i, l],
                 device_id=dev(sp=((z + d) % n_z) * 2 + k),
             )
-            for d in range(1, n_z)
+            for d in sorted(range(1, n_z), key=lambda d: (abs(2 * d - n_z), -d))
         ]
         res.append(
             pltpu.make_async_remote_copy(
@@ -214,19 +214,24 @@
             device_id=dev(sp=(me + 1) % n_sp),
         )
 
-    def project(l, c):
+    def norm(l, c):
         r = rows(c)
         total = jnp.zeros((t_rows, 1), F32)
         for p in range(n_tp):
             v = xs[l, p, r, :].astype(F32)
             total = total + jnp.sum(v * v, axis=1, keepdims=True)
         rs = lax.rsqrt(total / (n_tp * cols) + EPS)
+        for p in range(n_tp):
+            v = xs[l, p, r, :].astype(F32)
+            g = gain[l : l + 1, p * cols : (p + 1) * cols].astype(F32)
+            nrm[p, r, :] = (v * rs * g).astype(BF16)
+
+    def project(l, c):
+        r = rows(c)
         xr = jnp.zeros((t_rows, ch), F32)
         gr = jnp.zeros((t_rows, ch), F32)
         for p in range(n_tp):
-            v = xs[l, p, r, :].astype(F32)
-            g = gain[l : l + 1, p * cols : (p + 1) * cols].astype(F32)
-            nv = (v * rs * g).astype(BF16)
+            nv = nrm[p, r, :]
             xr += jnp.dot(nv, wx[l, p * cols : (p + 1) * cols, :], preferred_element_type=F32)
             gr += jnp.dot(nv, wg[l, p * cols : (p + 1) * cols, :], preferred_element_type=F32)
         xp[l, pl.ds(pl.multiple_of(c * t_rows + PAD, 8), t_rows), :] = xr.astype(BF16).astype(F32)
@@ -312,38 +317,47 @@
         def front(i, carry):
             c = chunks - 1 - i
 
-            @pl.when(i < chunks)
-            def _():
-                near(0, l, c)
-                if l == 0:
-                    @pl.when(c >= 2)
-                    def _():
-                        send_own(0, 0, c - 2)
-
-            @pl.when(i == 1)
-            def _():
-                w_forward(0, l)
-                w_forward(1, l)
-                w_issue(2, l)
-                w_ready(0, l)
-                w_ready(1, l)
+            near(0, l, c)
+            if l == 0:
+                @pl.when(c >= 2)
+                def _():
+                    send_own(0, 0, c - 2)
 
             @pl.when(i >= 1)
             def _():
                 farther(0, l, c + 1)
-                project(l, c + 1)
-
-            @pl.when((i == 1) & (me < n_sp - 1))
+                norm(l, c + 1)
+
+            return carry
+
+        lax.fori_loop(0, chunks, front, 0)
+        w_forward(0, l)
+        w_forward(1, l)
+        w_issue(2, l)
+        w_ready(0, l)
+        w_ready(1, l)
+
+        def middle(i, carry):
+            c = chunks - 1 - i
+
+            @pl.when(i == chunks - 1)
+            def _():
+                farther(0, l, 0)
+                norm(l, 0)
+
+            project(l, c)
+
+            @pl.when((i == 0) & (me < n_sp - 1))
             def _():
                 rim_copy(l).start()
 
-            @pl.when(i >= 2)
+            @pl.when(i >= 1)
             def _():
-                gates(l, c + 2)
+                gates(l, c + 1)
 
             return carry
 
-        lax.fori_loop(0, chunks + 1, front, 0)
+        lax.fori_loop(0, chunks, middle, 0)
 
         @pl.when(me > 0)
         def _():
@@ -457,6 +471,7 @@
         in_specs=[hb, vm, hb, hb, vm, vm, vm, vm, vm, vm, hb],
         out_specs=vm,
         scratch_shapes=[
+            pltpu.VMEM((n_tp, tok_rows, cols), BF16),
             pltpu.VMEM((layers, n_tp, tok_rows, cols), BF16),
             pltpu.VMEM((layers, n_tp, tok_rows, ch), BF16),
             pltpu.VMEM((layers, d, ch), BF16),

time: 117 us -> 129 us (1.10)
  the two profiles are of different devices: /device:TPU:24 before, /device:TPU:0 now
where the time goes in v3:
time: 129 us
  Pallas kernels  125 us (97%)
  local copies, waits for them, and re-layouts  3.71 us (3%)
    pallas_call x1, Pallas kernels, body(): pl.pallas_call(functools.partial(kernel, (n_sp, n_tp, layers, chunks)), o...  125 us

profile of v3, /device:TPU:0, one launch (start us, length us, event | category | flops | bytes accessed | tf_op | source)
XLA Modules:
  0.0 129.0 jit_solution(13498520168147834067)
XLA Ops:
  0.0 0.0 copy-start
  0.0 0.7 stack.9
  0.7 0.0 copy-done
  0.7 0.9 copy.15.pj
  1.7 125.3 %shard_map.118 = bf16[768,512]{1,0:T(8,128)(2,1)} custom-call(bf16[768,512]{1,0:T(8,128)(2,1)} %tokens.1, bf16[2,2048]{1,0:T(2,128)(2,1)} %gain.1, bf16[2,256,256]{2,1,0:T(8,128)(2,1)} %xw.1, bf16[2,256,256]{2,1,0:T(8,128)(2,1)} %gw.1, bf16[2,4,256]{2,1,0:T(4,128)(2,1)} %taps.1, bf16[2,4,64,64]{3,2,1,0:T(8,128)(2,1)} %am.1, bf16[2,4,64,64]{3,2,1,0:T(8,128)(2,1)} %im.1, ...), custom_call_target="tpu_custom_call" | custom-call | tf_op jit(solution)/shard_map/pallas_call | solution.py:468
  127.0 2.1 %copy.17 = bf16[768,512]{1,0:T(8,128)(2,1)} copy(bf16[768,512]{1,0:T(8,128)(2,1)} %shard_map.118) | data formatting | bytes 1572864
  (2 shorter events, 0.0 us)
Async XLA Ops:
  0.0 0.7 copy-start
